TPU v7x, 32 devices: a whole 2x2x4 slice. The times are simulated.
32 devices in a mesh: sp: 8 (over z, y), tp: 4 (over x, core).
Axes of the slice: x: 2, y: 2, z: 4, core: 2. Of those that a mesh axis runs over, the one named last changes fastest.
Arguments:
- tokens: bfloat16 [6144, 2048], P('sp'), may hold values from -6 to 6
- input_gain: bfloat16 [2048], replicated, may hold values from 0.099609375 to 1.8984375
- gate_weight: bfloat16 [2048, 2048], P('sp', 'tp'), may hold values from -0.125 to 0.125
- value_weight: bfloat16 [2048, 2048], P('sp', 'tp'), may hold values from -0.125 to 0.125
- inflow_weight: bfloat16 [2048, 4, 128], P('sp', 'tp'), may hold values from -0.125 to 0.125
- readout_weight: bfloat16 [2048, 4, 128], P('sp', 'tp'), may hold values from -0.125 to 0.125
- step_weight: bfloat16 [2048, 2, 32], P('sp', None, 'tp'), may hold values from -0.125 to 0.125
- conv_values: bfloat16 [5, 2048], P(None, 'tp'), may hold values from -2.5 to 2.5
- conv_inflow: bfloat16 [5, 4, 128], P(None, 'tp'), may hold values from -2.5 to 2.5
- conv_readout: bfloat16 [5, 4, 128], P(None, 'tp'), may hold values from -2.5 to 2.5
- log_rate: float32 [2, 6144, 32], P(None, 'sp', 'tp'), may hold values from -20 to 0
- group_gain: bfloat16 [2048], P('tp'), may hold values from 0.099609375 to 1.8984375
- query_weight: bfloat16 [2048, 2048], P('sp', 'tp'), may hold values from -8 to 8
- key_weight: bfloat16 [2048, 512], P('sp', 'tp'), may hold values from -8 to 8
- vector_weight: bfloat16 [2048, 512], P('sp', 'tp'), may hold values from -0.125 to 0.125
- sink_logit: float32 [32], P('tp'), may hold values from 3 to 7
- state_out: bfloat16 [2048, 2048], P('tp', 'sp'), may hold values from -0.125 to 0.125
- window_out: bfloat16 [2048, 2048], P('tp', 'sp'), may hold values from -1 to 1
Outputs:
- mixed: bfloat16 [6144, 2048], P('sp', 'tp')
- log_total: float32 [6144, 32], P('sp', 'tp')
All inputs are finite; a program needn't handle non-finite values.
Results may differ from a plain program's by a relative error of at most 0.015.
The roundings to bfloat16 on the way count: a program that leaves them out, or rounds other values in their place, can miss the bound.
Values may be sent and summed in bfloat16 or wider, within the bound.
A program may use at most 128 MiB of HBM per device.

v0:
```python
import functools

import jax
import jax.numpy as jnp
import numpy as np
from jax import lax
from jax.experimental import pallas as pl
from jax.experimental.pallas import tpu as pltpu
from jax.sharding import PartitionSpec as P


HEAD_DIM = 64
CONV = 5
SSD_BLOCK = 128
WINDOW = 128
GRID_W = 64


EPS = 1e-06
ROPE_BASE = 10000.0
HIGHEST = lax.Precision.HIGHEST
F32 = jnp.float32
BF16 = jnp.bfloat16
PAD = 16


def iota(shape, dim):
    return lax.broadcasted_iota(jnp.int32, shape, dim)


def exact(a, b):
    return jnp.dot(a, b, precision=HIGHEST, preferred_element_type=F32)


def spread(heads):
    shape = (heads, heads * HEAD_DIM)
    return (iota(shape, 1) // HEAD_DIM == iota(shape, 0)).astype(F32)


def inner_t(a, b):
    return lax.dot_general(a, b, (((1,), (1,)), ((), ())), preferred_element_type=F32)


def outer_t(a, b):
    return lax.dot_general(a, b, (((0,), (0,)), ((), ())), preferred_element_type=F32)


def summary_kernel(cells_ref, sd_ref, out_ref):
    count = cells_ref.shape[0]
    heads = sd_ref.shape[1] // 4
    wide = heads * HEAD_DIM
    state = out_ref.shape[1] - PAD
    x = cells_ref[:, :wide].astype(F32)
    writes = cells_ref[:, wide : wide + state]
    expand = spread(heads)
    row = iota((count, count), 0)
    col = iota((count, count), 1)
    for e in range(2):
        step = sd_ref[:, e * heads : (e + 1) * heads]
        decay = sd_ref[:, (2 + e) * heads : (3 + e) * heads]
        span = (col > row) if e == 0 else (col < row)
        rest = exact(span.astype(F32), decay)
        scaled = (x * exact(jnp.exp(rest) * step, expand)).astype(BF16)
        out_ref[e, :state, :] = outer_t(writes, scaled).astype(BF16)
        total = exact(jnp.broadcast_to(jnp.sum(decay, axis=0, keepdims=True), (8, heads)), expand)
        total = total[0:1]
        high = total.astype(BF16).astype(F32)
        place = iota((PAD, wide), 0)
        packed = jnp.where(place == 0, high, jnp.where(place == 1, total - high, 0.0))
        out_ref[e, state:, :] = packed.astype(BF16)


def mixer_kernel(cells_ref, sd_ref, sdt_ref, start_ref, gate_ref, gain_ref, out_ref, back_ref, carry_ref):
    blocks, _, size = sdt_ref.shape
    heads = sd_ref.shape[1] // 4
    wide = heads * HEAD_DIM
    state = start_ref.shape[1]
    expand = spread(heads)
    row = iota((size, size), 0)
    col = iota((size, size), 1)
    lower = (row >= col).astype(F32)
    upper = (row <= col).astype(F32)

    carry_ref[...] = start_ref[1]

    def backward(index, _):
        block = blocks - 1 - index
        rows = pl.ds(pl.multiple_of(block * size, size), size)
        back_ref[block] = carry_ref[...].astype(BF16)
        step = sd_ref[rows, heads : 2 * heads]
        cum = exact(upper, sd_ref[rows, 3 * heads : 4 * heads])
        edge = cum[0:1]
        x = cells_ref[rows, :wide].astype(F32)
        scaled = (x * exact(jnp.exp(edge - cum) * step, expand)).astype(BF16)
        fresh = outer_t(cells_ref[rows, wide : wide + state], scaled)
        fade = exact(jnp.broadcast_to(jnp.exp(edge), (8, heads)), expand)[0:1]
        carry_ref[...] = fade * carry_ref[...] + fresh
        return 0

    lax.fori_loop(0, blocks, backward, 0)
    carry_ref[...] = start_ref[0]

    def forward(block, _):
        rows = pl.ds(pl.multiple_of(block * size, size), size)
        cum_f = exact(lower, sd_ref[rows, 2 * heads : 3 * heads])
        cum_b = exact(upper, sd_ref[rows, 3 * heads : 4 * heads])
        flat = sdt_ref[block]
        step_ft = flat[:heads]
        step_bt = flat[heads : 2 * heads]
        cum_ft = exact(flat[2 * heads : 3 * heads], upper)
        cum_bt = exact(flat[3 * heads :], lower)
        x = cells_ref[rows, :wide]
        writes = cells_ref[rows, wide : wide + state]
        reads = cells_ref[rows, wide + state :]
        cross = inner_t(reads, writes)
        parts = []
        for h in range(heads):
            one = slice(h, h + 1)
            seg = jnp.where(
                row >= col, cum_f[:, one] - cum_ft[one], cum_b[:, one] - cum_bt[one]
            )
            scale = jnp.where(
                row > col,
                step_ft[one],
                jnp.where(row < col, step_bt[one], step_ft[one] + step_bt[one]),
            )
            weight = (cross * jnp.exp(seg) * scale).astype(BF16)
            parts.append(
                jnp.dot(
                    weight, x[:, h * HEAD_DIM : (h + 1) * HEAD_DIM], preferred_element_type=F32
                )
            )
        y = jnp.concatenate(parts, axis=1)
        y = y + exact(jnp.exp(cum_f), expand) * jnp.dot(
            reads, carry_ref[...].astype(BF16), preferred_element_type=F32
        )
        y = y + exact(jnp.exp(cum_b), expand) * jnp.dot(
            reads, back_ref[block], preferred_element_type=F32
        )
        gate = gate_ref[rows, :].astype(F32)
        y = y * (gate * jax.nn.sigmoid(gate))
        y = y * lax.rsqrt(jnp.mean(y * y, axis=1, keepdims=True) + EPS)
        out_ref[rows, :] = (y * gain_ref[...].astype(F32)).astype(BF16)
        edge = cum_f[size - 1 : size]
        step = sd_ref[rows, :heads]
        scaled = (x.astype(F32) * exact(jnp.exp(edge - cum_f) * step, expand)).astype(BF16)
        fade = exact(jnp.broadcast_to(jnp.exp(edge), (8, heads)), expand)[0:1]
        carry_ref[...] = fade * carry_ref[...] + outer_t(writes, scaled)
        return 0

    lax.fori_loop(0, blocks, forward, 0)


def attend_kernel(place_ref, sink_ref, q_ref, kv_ref, turn_ref, swap_ref, out_ref, log_ref, keys_ref):
    count = q_ref.shape[0]
    q_count = q_ref.shape[1] // HEAD_DIM
    kv_width = kv_ref.shape[1] // 2
    repeat = q_count * HEAD_DIM // kv_width
    size = SSD_BLOCK
    band = size + 2 * WINDOW
    swap = swap_ref[...]

    def turned(part, rows):
        swapped = jnp.dot(part, swap, preferred_element_type=F32)
        table = turn_ref[rows, :]
        return (part.astype(F32) * table[:, :HEAD_DIM] + swapped * table[:, HEAD_DIM:]).astype(BF16)

    def prepare(block, _):
        rows = pl.ds(pl.multiple_of(block * size, size), size)
        for g in range(kv_width // HEAD_DIM):
            keys_ref[g, rows, :] = turned(
                kv_ref[rows, g * HEAD_DIM : (g + 1) * HEAD_DIM], rows
            )
        return 0

    lax.fori_loop(0, kv_ref.shape[0] // size, prepare, 0)
    row = iota((size, band), 0)
    col = iota((size, band), 1)
    near = (col >= row) & (col - row <= 2 * WINDOW)
    lane = iota((size, q_count), 1)

    def one(block, _):
        start = pl.multiple_of(block * size, size)
        rows = pl.ds(start, size)
        reach = pl.ds(start, band)
        key_pos = place_ref[0] + start - WINDOW + col
        valid = near & (key_pos >= 0) & (key_pos < place_ref[1])
        logs = jnp.zeros((size, q_count), F32)
        outs = []
        for h in range(q_count):
            g = h // repeat
            query = turned(
                q_ref[rows, h * HEAD_DIM : (h + 1) * HEAD_DIM], pl.ds(start + WINDOW, size)
            )
            scores = inner_t(query, keys_ref[g, reach, :]) * HEAD_DIM ** (-0.5)
            scores = jnp.where(valid, scores, -jnp.inf)
            sink = sink_ref[h]
            top = jnp.maximum(jnp.max(scores, axis=1, keepdims=True), sink)
            expo = jnp.exp(scores - top)
            total = jnp.sum(expo, axis=1, keepdims=True) + jnp.exp(sink - top)
            first = kv_width + g * HEAD_DIM
            values = jnp.dot(
                expo.astype(BF16),
                kv_ref[reach, first : first + HEAD_DIM],
                preferred_element_type=F32,
            )
            outs.append((values / total).astype(BF16))
            logs = jnp.where(lane == h, top + jnp.log(total), logs)
        out_ref[rows, :] = jnp.concatenate(outs, axis=1)
        log_ref[rows, :] = logs
        return 0

    lax.fori_loop(0, count // size, one, 0)


def call(kernel, out_shape, args, scratch=(), scalars=0, flops=10**8):
    vmem = pl.BlockSpec(memory_space=pltpu.VMEM)
    smem = pl.BlockSpec(memory_space=pltpu.SMEM)
    return pl.pallas_call(
        kernel,
        out_shape=out_shape,
        in_specs=[smem] * scalars + [vmem] * (len(args) - scalars),
        out_specs=jax.tree.map(lambda _: vmem, out_shape),
        scratch_shapes=list(scratch),
        cost_estimate=pl.CostEstimate(flops=flops, bytes_accessed=4 * 10**6, transcendentals=0),
        compiler_params=pltpu.CompilerParams(vmem_limit_bytes=40 * 2**20),
    )(*args)


def with_halo(cells, sides, width):
    for axis, dim in sides:
        count = lax.axis_size(axis)
        ends = count - 1
        head = lax.slice_in_dim(cells, 0, width, axis=dim)
        tail = lax.slice_in_dim(cells, cells.shape[dim] - width, cells.shape[dim], axis=dim)
        cells = jnp.concatenate(
            [
                lax.ppermute(tail, axis, [(i, (i + 1) % count) for i in range(ends)]),
                cells,
                lax.ppermute(head, axis, [((i + 1) % count, i) for i in range(ends)]),
            ],
            axis=dim,
        )
    return cells


def flatten_rows(weight):
    return weight.reshape(weight.shape[0], -1)


TILE = 128
GROUP = 3


def split3(v):
    high = v.astype(BF16)
    rest = v - high.astype(F32)
    mid = rest.astype(BF16)
    return high, mid, (rest - mid.astype(F32)).astype(BF16)


def through(left, right, left_wide):
    total = None
    for part in split3(left if left_wide else right):
        one = jnp.dot(part, right, preferred_element_type=F32) if left_wide else jnp.dot(
            left, part, preferred_element_type=F32
        )
        total = one if total is None else total + one
    return total


def chunk_maps(shapes):
    rows = shapes["value"][0]

    def tiles(name):
        return [(name, 0, c) for c in range(shapes[name][1] // TILE)]

    units = ([], [])
    for names in (("value", "inflow", "readout"), ("query", "key", "vector"), ("gate",)):
        flat = [t for name in names for t in tiles(name)]
        half = len(flat) // 2
        for d in range(2):
            units[d].extend(flat[d * half : (d + 1) * half])
    for d in range(2):
        for name in ("state_out", "window_out"):
            units[d].extend((name, r, d) for r in range(shapes[name][0] // rows))
    return units


def layer_kernel(
    cfg,
    tokens_ref,
    gain_ref,
    taps_ref,
    rates_ref,
    norm_gain_ref,
    sink_ref,
    row_turn_ref,
    col_turn_ref,
    steps_ref,
    value_ref,
    inflow_ref,
    readout_ref,
    query_ref,
    key_ref,
    vector_ref,
    gate_w_ref,
    state_out_ref,
    window_out_ref,
    out_ref,
    log_ref,
    ring_ref,
    steps_all_ref,
    normed_ref,
    conv_ref,
    cells_ref,
    step_ref,
    decay_ref,
    cum_ref,
    entry_ref,
    before_ref,
    carry_ref,
    total_ref,
    scan_send_ref,
    scan_recv_ref,
    start_ref,
    reach_ref,
    gate_ref,
    q_ref,
    kv_ref,
    keys_ref,
    turn_ref,
    feat_ref,
    part_ref,
    peer_ref,
    send_sem,
    recv_sem,
    steps_send,
    steps_recv,
    local_sem,
    halo_send,
    halo_recv,
    kv_send,
    kv_recv,
    scan_ssem,
    scan_rsem,
    out_send,
    out_recv,
):
    seats, peers, units = cfg
    count, _ = tokens_ref.shape
    unit_rows = ring_ref.shape[3]
    heads = steps_ref.shape[0] // 2
    wide = heads * HEAD_DIM
    state = inflow_ref.shape[1]
    conv_width = wide + 2 * state
    q_width = query_ref.shape[1]
    q_count = q_width // HEAD_DIM
    kv_width = key_ref.shape[1]
    per_dir = len(units[0])
    hops = seats - 1
    sends = per_dir * hops
    place = lax.axis_index("sp")
    lane_peer = lax.axis_index("tp")
    half = seats // 2
    blocks = count // SSD_BLOCK
    size = SSD_BLOCK
    mesh_id = pl.DeviceIdType.MESH

    def seat_at(pos):
        pos = lax.rem(pos + 2 * seats, seats)
        late = lax.div(pos, half)
        return (1 - late) * 2 * pos + late * (2 * (seats - 1 - pos) + 1)

    odd = lax.rem(place, 2)
    my_pos = (1 - odd) * lax.div(place, 2) + odd * (seats - 1 - lax.div(place, 2))
    nexts = (seat_at(my_pos + 1), seat_at(my_pos - 1))

    barrier = pltpu.get_barrier_semaphore()
    for r in range(1, seats):
        pl.semaphore_signal(
            barrier, inc=1, device_id={"sp": lax.rem(place + r, seats)}, device_id_type=mesh_id
        )
    for r in range(1, peers):
        pl.semaphore_signal(
            barrier, inc=1, device_id={"tp": lax.rem(lane_peer + r, peers)}, device_id_type=mesh_id
        )

    sources = {
        "value": value_ref,
        "inflow": inflow_ref,
        "readout": readout_ref,
        "query": query_ref,
        "key": key_ref,
        "vector": vector_ref,
        "gate": gate_w_ref,
        "state_out": state_out_ref,
        "window_out": window_out_ref,
    }
    locals_ = []
    for d in range(2):
        for u, (name, r, c) in enumerate(units[d]):
            locals_.append(
                pltpu.make_async_copy(
                    sources[name].at[pl.ds(r * unit_rows, unit_rows), pl.ds(c * TILE, TILE)],
                    ring_ref.at[d, u, place],
                    local_sem.at[d * per_dir + u],
                )
            )
    for copy in locals_:
        copy.start()
    steps_all_ref[place] = steps_ref[...]
    for copy in locals_:
        copy.wait()
    pl.semaphore_wait(barrier, hops + peers - 1)

    def ring_copy(i, d, behind):
        turn = lax.div(i, GROUP * hops)
        k = lax.rem(lax.div(i, GROUP), hops) + behind
        unit = GROUP * turn + lax.rem(i, GROUP)
        owner = seat_at(my_pos - k) if d == 0 else seat_at(my_pos + k)
        block = ring_ref.at[d, unit, owner]
        return pltpu.make_async_remote_copy(
            src_ref=block,
            dst_ref=block,
            send_sem=send_sem.at[d, i],
            recv_sem=recv_sem.at[d, i],
            device_id={"sp": nexts[d]},
            device_id_type=mesh_id,
        )

    def tick(i, last=False):
        for d in range(2):
            ring_copy(i, d, 1).wait_recv()
            if not last:
                ring_copy(i + GROUP, d, 0).start()

    for j in range(GROUP):
        for d in range(2):
            ring_copy(jnp.int32(j), d, 0).start()

    def steps_copy(r):
        return pltpu.make_async_remote_copy(
            src_ref=steps_ref,
            dst_ref=steps_all_ref.at[place],
            send_sem=steps_send.at[r],
            recv_sem=steps_recv.at[place],
            device_id={"sp": lax.rem(place + r, seats)},
            device_id_type=mesh_id,
        )

    for r in range(1, seats):
        steps_copy(r).start()

    clock = [0]

    def sweep(trips, per_trip, body):
        base = clock[0]

        def run(i, _):
            for j in range(per_trip):
                tick(base + i * per_trip + j)
            body(i)
            return 0

        lax.fori_loop(0, trips, run, 0)
        clock[0] = base + trips * per_trip

    def until(goal):
        if goal > clock[0]:
            sweep(goal - clock[0], 1, lambda i: None)

    def rows_at(index, length, first=0):
        return pl.ds(pl.multiple_of(index * length, length) + first, length)

    def normalise(b):
        rows = rows_at(b, size)
        x = tokens_ref[rows, :].astype(F32)
        scale = lax.rsqrt(jnp.mean(x * x, axis=1, keepdims=True) + EPS)
        normed_ref[rows, :] = (x * scale * gain_ref[...].astype(F32)).astype(BF16)

    sweep(blocks, 0, normalise)
    table_row = place * (count // GRID_W)

    def fill_turn(i):
        turn_ref[rows_at(i, GRID_W), :] = col_turn_ref[...] + row_turn_ref[pl.ds(table_row + i, 1), :]

    sweep(turn_ref.shape[0] // GRID_W, 0, fill_turn)
    step_ref[...] = jnp.zeros_like(step_ref)
    carry_ref[...] = jnp.zeros_like(carry_ref)
    total_ref[...] = jnp.zeros_like(total_ref)
    start_ref[...] = jnp.zeros_like(start_ref)
    reach_ref[...] = jnp.zeros_like(reach_ref)

    first_edge = place == 0
    last_edge = place == seats - 1

    @pl.when(first_edge)
    def _():
        conv_ref[:PAD, :] = jnp.zeros((PAD, conv_width), BF16)
        kv_ref[:WINDOW, :] = jnp.zeros((WINDOW, 2 * kv_width), BF16)

    @pl.when(last_edge)
    def _():
        conv_ref[PAD + count :, :] = jnp.zeros((PAD, conv_width), BF16)
        kv_ref[WINDOW + count :, :] = jnp.zeros((WINDOW, 2 * kv_width), BF16)

    def weights(d, first, last):
        return jnp.concatenate(
            [ring_ref[d, u].reshape(seats * unit_rows, TILE) for u in range(first, last)], axis=1
        )

    first_units = conv_width // (2 * TILE)
    second_units = (q_width + 2 * kv_width) // (2 * TILE)
    gate_units = wide // (2 * TILE)
    until(GROUP * hops * -(-first_units // GROUP))
    for r in range(1, seats):
        peer = lax.rem(place + r, seats)
        pltpu.make_async_remote_copy(
            src_ref=steps_ref,
            dst_ref=steps_all_ref.at[peer],
            send_sem=steps_send.at[r],
            recv_sem=steps_recv.at[peer],
            device_id={"sp": peer},
            device_id_type=mesh_id,
        ).wait_recv()

    dot_rows = 2 * size

    def first_dot(b):
        rows = rows_at(b, dot_rows)
        here = normed_ref[rows, :]
        for d in range(2):
            conv_ref[rows_at(b, dot_rows, PAD), d * first_units * TILE : (d + 1) * first_units * TILE] = (
                jnp.dot(here, weights(d, 0, first_units), preferred_element_type=F32).astype(BF16)
            )
        steps = jnp.concatenate([steps_all_ref[o] for o in range(seats)], axis=1)
        raw = inner_t(here, steps)
        step = jnp.maximum(raw, 0.0) + jnp.log1p(jnp.exp(-jnp.abs(raw)))
        step_ref[rows, : 2 * heads] = step

    sweep(count // dot_rows, 1, first_dot)

    def edge_copies(ref, length, ssem, rsem):
        inner = ref.shape[0] - 2 * length
        up = pltpu.make_async_remote_copy(
            src_ref=ref.at[pl.ds(inner, length)],
            dst_ref=ref.at[pl.ds(0, length)],
            send_sem=ssem.at[0],
            recv_sem=rsem.at[0],
            device_id={"sp": lax.rem(place + 1, seats)},
            device_id_type=mesh_id,
        )
        down = pltpu.make_async_remote_copy(
            src_ref=ref.at[pl.ds(length, length)],
            dst_ref=ref.at[pl.ds(length + inner, length)],
            send_sem=ssem.at[1],
            recv_sem=rsem.at[1],
            device_id={"sp": lax.rem(place + hops, seats)},
            device_id_type=mesh_id,
        )
        return up, down

    def edges_start(pair):
        pl.when(jnp.logical_not(last_edge))(lambda: pair[0].start())
        pl.when(jnp.logical_not(first_edge))(lambda: pair[1].start())

    def edges_arrive(pair):
        pl.when(jnp.logical_not(first_edge))(lambda: pair[0].wait_recv())
        pl.when(jnp.logical_not(last_edge))(lambda: pair[1].wait_recv())

    def edges_left(pair):
        pl.when(jnp.logical_not(last_edge))(lambda: pair[0].wait_send())
        pl.when(jnp.logical_not(first_edge))(lambda: pair[1].wait_send())

    conv_edges = edge_copies(conv_ref, PAD, halo_send, halo_recv)
    edges_start(conv_edges)
    decay_ref[...] = rates_ref[...] * step_ref[...]
    lane = iota((size, TILE), 1)
    row = iota((size, size), 0)
    col = iota((size, size), 1)
    lower = (row >= col).astype(BF16)
    upper = (row <= col).astype(BF16)
    spread_row = iota((TILE, wide), 0)
    spread_col = iota((TILE, wide), 1) // HEAD_DIM
    spreads = [(spread_row - e * heads == spread_col).astype(BF16) for e in range(2)]

    def sums(b):
        rows = rows_at(b, size)
        decay = decay_ref[rows, :]
        cum_ref[rows, :] = jnp.where(
            lane < heads, through(lower, decay, False), through(upper, decay, False)
        )

    sweep(blocks, 0, sums)
    edges_arrive(conv_edges)

    def convolve(b):
        rows = rows_at(b, size)
        padded = conv_ref[pl.ds(pl.multiple_of(b * size, size), size + 2 * PAD), :].astype(F32)
        first = PAD - CONV // 2
        taps = taps_ref[...].astype(F32)
        total = padded[first : first + size] * taps[0:1]
        for tap in range(1, CONV):
            total = total + padded[first + tap : first + tap + size] * taps[tap : tap + 1]
        cells_ref[rows, :] = (total * jax.nn.sigmoid(total)).astype(BF16)

    sweep(blocks, 1, convolve)

    def summarise(i):
        for e in range(2):
            b = i if e == 0 else blocks - 1 - i
            rows = rows_at(b, size)
            cum = cum_ref[rows, :]
            edge = cum[size - 1 : size] if e == 0 else cum[0:1]
            scale = through(jnp.exp(edge - cum) * step_ref[rows, :], spreads[e], True)
            scaled = (cells_ref[rows, :wide].astype(F32) * scale).astype(BF16)
            fresh = outer_t(cells_ref[rows, wide : wide + state], scaled)
            edges = through(jnp.broadcast_to(edge, (8, TILE)), spreads[e], True)
            entry_ref[e, b] = carry_ref[e]
            before_ref[e, b] = total_ref[e]
            carry_ref[e] = jnp.exp(edges[0:1]) * carry_ref[e] + fresh
            total_ref[e] = total_ref[e] + edges

    sweep(blocks, 2, summarise)

    jumps = [1]
    while sum(jumps) < hops:
        jumps.append(sum(jumps))

    def scan_copy(r, e):
        step = jumps[r] if e == 0 else seats - jumps[r]
        return pltpu.make_async_remote_copy(
            src_ref=scan_send_ref.at[e, r],
            dst_ref=scan_recv_ref.at[e, r],
            send_sem=scan_ssem.at[e, r],
            recv_sem=scan_rsem.at[e, r],
            device_id={"sp": lax.rem(place + step, seats)},
            device_id_type=mesh_id,
        )

    def sends_to(r, e):
        return place < seats - jumps[r] if e == 0 else place >= jumps[r]

    def hears_from(r, e):
        return place >= jumps[r] if e == 0 else place < seats - jumps[r]

    def scan_start(r, state_ref, decay_sum_ref):
        for e in range(2):
            scan_send_ref[e, r, :state] = state_ref[e].astype(BF16)
            total = decay_sum_ref[e][0:1]
            high = total.astype(BF16).astype(F32)
            at = iota((PAD, wide), 0)
            scan_send_ref[e, r, state:] = jnp.where(
                at == 0, high, jnp.where(at == 1, total - high, 0.0)
            ).astype(BF16)
            pl.when(sends_to(r, e))(lambda: scan_copy(r, e).start())

    def scan_take(r):
        for e in range(2):

            @pl.when(hears_from(r, e))
            def _():
                scan_copy(r, e).wait_recv()
                far = scan_recv_ref[e, r]
                decays = far[state : state + 8].astype(F32)
                far_total = decays[0:1] + decays[1:2]
                start_ref[e] = (
                    far[:state].astype(F32) * jnp.exp(reach_ref[e][0:1]) + start_ref[e]
                )
                reach_ref[e] = reach_ref[e] + far_total

    scan_start(0, carry_ref, total_ref)

    until(GROUP * hops * -(-(first_units + second_units) // GROUP))

    q_last = second_units - 2 * kv_width // TILE

    def second_dot_b(b):
        rows = rows_at(b, dot_rows)
        got = jnp.dot(
            normed_ref[rows, :],
            weights(1, first_units, first_units + second_units),
            preferred_element_type=F32,
        ).astype(BF16)
        q_ref[rows, second_units * TILE :] = got[:, : q_last * TILE]
        kv_ref[rows_at(b, dot_rows, WINDOW), :] = got[:, q_last * TILE :]

    sweep(count // dot_rows, 1, second_dot_b)
    kv_edges = edge_copies(kv_ref, WINDOW, kv_send, kv_recv)
    edges_start(kv_edges)
    scan_take(0)
    scan_start(1, start_ref, reach_ref)

    def second_dot_a(b):
        rows = rows_at(b, dot_rows)
        q_ref[rows, : second_units * TILE] = jnp.dot(
            normed_ref[rows, :],
            weights(0, first_units, first_units + second_units),
            preferred_element_type=F32,
        ).astype(BF16)

    sweep(count // dot_rows, 1, second_dot_a)

    quarter = HEAD_DIM // 4
    low = lax.rem(iota((size, TILE), 1), 2 * quarter) < quarter

    def turned(part, table):
        x = part.astype(F32)
        other = jnp.where(low, pltpu.roll(x, TILE - quarter, 1), pltpu.roll(x, quarter, 1))
        return (x * table[:, :TILE] + other * table[:, TILE:]).astype(BF16)

    edges_arrive(kv_edges)

    def prepare(b):
        rows = rows_at(b, size)
        for c in range(kv_width // TILE):
            keys_ref[rows, c * TILE : (c + 1) * TILE] = turned(
                kv_ref[rows, c * TILE : (c + 1) * TILE], turn_ref[rows, :]
            )

    sweep(kv_ref.shape[0] // size, 0, prepare)

    band = size + 2 * WINDOW
    band_row = iota((size, band), 0)
    band_col = iota((size, band), 1)
    near = (band_col >= band_row) & (band_col - band_row <= 2 * WINDOW)
    q_lane = iota((size, q_count), 1)
    repeat = q_count * HEAD_DIM // kv_width
    seq_total = seats * count
    later = [1, 3, 5]

    def attend(b):
        for r in range(1, len(jumps)):

            @pl.when(b == later[r - 1])
            def _():
                scan_take(r)
                if r + 1 < len(jumps):
                    scan_start(r + 1, start_ref, reach_ref)

        start = pl.multiple_of(b * size, size)
        rows = pl.ds(start, size)
        reach = pl.ds(start, band)
        key_pos = place * count + start - WINDOW + band_col
        valid = near & (key_pos >= 0) & (key_pos < seq_total)
        logs = jnp.zeros((size, q_count), F32)
        table = turn_ref[pl.ds(start + WINDOW, size), :]
        turned_q = jnp.concatenate(
            [turned(q_ref[rows, c * TILE : (c + 1) * TILE], table) for c in range(q_width // TILE)],
            axis=1,
        )
        outs = []
        for h in range(q_count):
            g = h // repeat
            scores = inner_t(
                turned_q[:, h * HEAD_DIM : (h + 1) * HEAD_DIM],
                keys_ref[reach, g * HEAD_DIM : (g + 1) * HEAD_DIM],
            ) * HEAD_DIM ** (-0.5)
            scores = jnp.where(valid, scores, -jnp.inf)
            sink = sink_ref[h]
            top = jnp.maximum(jnp.max(scores, axis=1, keepdims=True), sink)
            expo = jnp.exp(scores - top)
            total = jnp.sum(expo, axis=1, keepdims=True) + jnp.exp(sink - top)
            begin = kv_width + g * HEAD_DIM
            values = jnp.dot(
                expo.astype(BF16),
                kv_ref[reach, begin : begin + HEAD_DIM],
                preferred_element_type=F32,
            )
            outs.append((values / total).astype(BF16))
            logs = jnp.where(q_lane == h, top + jnp.log(total), logs)
        feat_ref[rows, wide:] = jnp.concatenate(outs, axis=1)
        log_ref[rows, :] = logs

    sweep(blocks, 3, attend)

    gate_first = first_units + second_units
    until(GROUP * hops * -(-(gate_first + gate_units) // GROUP))

    def gate_dot(b):
        rows = rows_at(b, dot_rows)
        for d in range(2):
            gate_ref[rows, d * gate_units * TILE : (d + 1) * gate_units * TILE] = jnp.dot(
                normed_ref[rows, :],
                weights(d, gate_first, gate_first + gate_units),
                preferred_element_type=F32,
            ).astype(BF16)

    sweep(count // dot_rows, 0, gate_dot)

    def mix(b):
        rows = rows_at(b, size)
        cum = cum_ref[rows, :]
        step = step_ref[rows, :]
        cum_t = cum.T
        step_t = step.T
        x = cells_ref[rows, :wide]
        writes = cells_ref[rows, wide : wide + state]
        reads = cells_ref[rows, wide + state :]
        cross = inner_t(reads, writes)
        parts = []
        for h in range(heads):
            f = slice(h, h + 1)
            g = slice(heads + h, heads + h + 1)
            seg = jnp.where(row >= col, cum[:, f] - cum_t[f], cum[:, g] - cum_t[g])
            scale = jnp.where(
                row > col, step_t[f], jnp.where(row < col, step_t[g], step_t[f] + step_t[g])
            )
            weight = (cross * jnp.exp(seg) * scale).astype(BF16)
            parts.append(
                jnp.dot(weight, x[:, h * HEAD_DIM : (h + 1) * HEAD_DIM], preferred_element_type=F32)
            )
        y = jnp.concatenate(parts, axis=1)
        fades = jnp.exp(cum)
        for e in range(2):
            held = entry_ref[e, b] + jnp.exp(before_ref[e, b][0:1]) * start_ref[e]
            y = y + through(fades, spreads[e], True) * jnp.dot(
                reads, held.astype(BF16), preferred_element_type=F32
            )
        gate = gate_ref[rows, :].astype(F32)
        y = y * (gate * jax.nn.sigmoid(gate))
        y = y * lax.rsqrt(jnp.mean(y * y, axis=1, keepdims=True) + EPS)
        feat_ref[rows, :wide] = (y * norm_gain_ref[...].astype(F32)).astype(BF16)

    left_ticks = sends - GROUP - clock[0]
    sweep(blocks, min(2, left_ticks // blocks), mix)

    out_first = gate_first + gate_units
    out_units = per_dir - out_first
    per_peer = 2 * seats // peers

    def out_copy(tile):
        dest = lax.div(tile, per_peer)
        return dest, pltpu.make_async_remote_copy(
            src_ref=part_ref.at[tile],
            dst_ref=peer_ref.at[lane_peer, lax.rem(tile, per_peer)],
            send_sem=out_send.at[tile],
            recv_sem=out_recv.at[lane_peer, lax.rem(tile, per_peer)],
            device_id={"tp": dest},
            device_id_type=mesh_id,
        )

    def project(d, owner):
        tile = 2 * owner + d
        matrix = ring_ref[d, out_first:, owner].reshape(out_units * unit_rows, TILE)

        def rows_dot(b, _):
            rows = rows_at(b, dot_rows)
            part_ref[tile, rows, :] = jnp.dot(
                feat_ref[rows, :], matrix, preferred_element_type=F32
            ).astype(BF16)
            return 0

        lax.fori_loop(0, count // dot_rows, rows_dot, 0)
        dest, copy = out_copy(tile)
        pl.when(dest != lane_peer)(lambda: copy.start())

    for d in range(2):
        project(d, place)
    final = sends - GROUP * hops
    done = max(0, (clock[0] - final) // GROUP)

    def project_hop(k):
        project(0, seat_at(my_pos - k - 1))
        project(1, seat_at(my_pos + k + 1))

    def early(k, _):
        project_hop(k)
        return 0

    lax.fori_loop(0, done, early, 0)
    until(final + GROUP * done)
    sweep(hops - 1 - done, GROUP, lambda i: project_hop(i + done))
    for j in range(GROUP):
        tick(jnp.int32(sends - GROUP + j), last=True)
    project_hop(jnp.int32(hops - 1))

    def gather_peers(r, _):
        source = lax.rem(lane_peer + r, peers)
        for j in range(per_peer):
            pltpu.make_async_remote_copy(
                src_ref=part_ref.at[j],
                dst_ref=peer_ref.at[source, j],
                send_sem=out_send.at[j],
                recv_sem=out_recv.at[source, j],
                device_id={"tp": source},
                device_id_type=mesh_id,
            ).wait_recv()
        return 0

    lax.fori_loop(1, peers, gather_peers, 0)

    def add_up(b, _):
        rows = rows_at(b, size)
        for j in range(per_peer):
            total = part_ref[lane_peer * per_peer + j, rows, :].astype(F32)
            for r in range(1, peers):
                total = total + peer_ref[lax.rem(lane_peer + r, peers), j, rows, :].astype(F32)
            out_ref[rows, j * TILE : (j + 1) * TILE] = total.astype(BF16)
        return 0

    lax.fori_loop(0, blocks, add_up, 0)

    edges_left(conv_edges)
    edges_left(kv_edges)
    for r in range(len(jumps)):
        for e in range(2):
            pl.when(sends_to(r, e))(lambda: scan_copy(r, e).wait_send())
    for r in range(1, seats):
        steps_copy(r).wait_send()

    def ring_left(i, _):
        for d in range(2):
            ring_copy(i, d, 0).wait_send()
        return 0

    lax.fori_loop(0, sends, ring_left, 0)

    def out_left(tile, _):
        dest, copy = out_copy(tile)
        pl.when(dest != lane_peer)(lambda: copy.wait_send())
        return 0

    lax.fori_loop(0, 2 * seats, out_left, 0)


def turn_tables(rows_total):
    quarter = HEAD_DIM // 4
    freqs = np.float32(ROPE_BASE) ** (-np.arange(quarter).astype(np.float32) / np.float32(quarter))
    border = WINDOW // GRID_W
    row_angle = (np.arange(rows_total + 2 * border) - border).astype(np.float32)[:, None] * freqs
    col_angle = np.arange(GRID_W).astype(np.float32)[:, None] * freqs

    def table(angle, first):
        zero = np.zeros_like(angle)
        cosine = np.cos(angle)
        sine = np.sin(angle)
        one = [cosine, cosine, zero, zero] if first else [zero, zero, cosine, cosine]
        two = [-sine, sine, zero, zero] if first else [zero, zero, -sine, sine]
        copies = TILE // HEAD_DIM
        return np.concatenate(one * copies + two * copies, axis=1).astype(np.float32)

    return table(row_angle, True), table(col_angle, False)


def streamed(
    tokens,
    input_gain,
    gate_weight,
    value_weight,
    inflow_weight,
    readout_weight,
    step_weight,
    conv_values,
    conv_inflow,
    conv_readout,
    log_rate,
    group_gain,
    query_weight,
    key_weight,
    vector_weight,
    sink_logit,
    state_out,
    window_out,
):
    count, width = tokens.shape
    seats = lax.axis_size("sp")
    peers = lax.axis_size("tp")
    heads = step_weight.shape[2]
    unit_rows = value_weight.shape[0]
    inflow = flatten_rows(inflow_weight)
    readout = flatten_rows(readout_weight)
    wide = value_weight.shape[1]
    state = inflow.shape[1]
    conv_width = wide + 2 * state
    q_width = query_weight.shape[1]
    kv_width = key_weight.shape[1]
    blocks = count // SSD_BLOCK
    taps = jnp.concatenate([conv_values, flatten_rows(conv_inflow), flatten_rows(conv_readout)], axis=1)
    rates = -jnp.exp(jnp.transpose(log_rate, (1, 0, 2)).reshape(count, 2 * heads))
    rates = jnp.pad(rates, ((0, 0), (0, TILE - 2 * heads)))
    steps = jnp.transpose(step_weight, (1, 2, 0)).reshape(2 * heads, unit_rows)
    row_turn, col_turn = turn_tables(seats * count // GRID_W)
    units = chunk_maps(
        {
            "value": value_weight.shape,
            "inflow": inflow.shape,
            "readout": readout.shape,
            "query": query_weight.shape,
            "key": key_weight.shape,
            "vector": vector_weight.shape,
            "gate": gate_weight.shape,
            "state_out": state_out.shape,
            "window_out": window_out.shape,
        }
    )
    per_dir = len(units[0])
    sends = per_dir * (seats - 1)
    rounds = 1
    while 2 ** (rounds - 1) < seats - 1:
        rounds += 1
    vmem = pl.BlockSpec(memory_space=pltpu.VMEM)
    smem = pl.BlockSpec(memory_space=pltpu.SMEM)
    hbm = pl.BlockSpec(memory_space=pltpu.HBM)
    dma = pltpu.SemaphoreType.DMA
    scratch = [
        pltpu.VMEM((2, per_dir, seats, unit_rows, TILE), BF16),
        pltpu.VMEM((seats, 2 * heads, unit_rows), BF16),
        pltpu.VMEM((count, width), BF16),
        pltpu.VMEM((count + 2 * PAD, conv_width), BF16),
        pltpu.VMEM((count, conv_width), BF16),
        pltpu.VMEM((count, TILE), F32),
        pltpu.VMEM((count, TILE), F32),
        pltpu.VMEM((count, TILE), F32),
        pltpu.VMEM((2, blocks, state, wide), F32),
        pltpu.VMEM((2, blocks, 8, wide), F32),
        pltpu.VMEM((2, state, wide), F32),
        pltpu.VMEM((2, 8, wide), F32),
        pltpu.VMEM((2, rounds, state + PAD, wide), BF16),
        pltpu.VMEM((2, rounds, state + PAD, wide), BF16),
        pltpu.VMEM((2, state, wide), F32),
        pltpu.VMEM((2, 8, wide), F32),
        pltpu.VMEM((count, wide), BF16),
        pltpu.VMEM((count, q_width), BF16),
        pltpu.VMEM((count + 2 * WINDOW, 2 * kv_width), BF16),
        pltpu.VMEM((count + 2 * WINDOW, kv_width), BF16),
        pltpu.VMEM((count + 2 * WINDOW, 2 * TILE), F32),
        pltpu.VMEM((count, wide + q_width), BF16),
        pltpu.VMEM((2 * seats, count, TILE), BF16),
        pltpu.VMEM((peers, 2 * seats // peers, count, TILE), BF16),
        dma((2, sends)),
        dma((2, sends)),
        dma((seats,)),
        dma((seats,)),
        dma((2 * per_dir,)),
        dma((2,)),
        dma((2,)),
        dma((2,)),
        dma((2,)),
        dma((2, rounds)),
        dma((2, rounds)),
        dma((2 * seats,)),
        dma((peers, 2 * seats // peers)),
    ]
    return pl.pallas_call(
        functools.partial(layer_kernel, (seats, peers, units)),
        out_shape=(
            jax.ShapeDtypeStruct((count, width // peers), BF16),
            jax.ShapeDtypeStruct((count, q_width // HEAD_DIM), F32),
        ),
        in_specs=[vmem] * 5 + [smem] + [vmem] * 3 + [hbm] * 9,
        out_specs=(vmem, vmem),
        scratch_shapes=scratch,
        compiler_params=pltpu.CompilerParams(
            collective_id=0, has_side_effects=True, vmem_limit_bytes=60 * 2**20
        ),
    )(
        tokens,
        input_gain[None],
        taps,
        rates,
        group_gain[None],
        sink_logit,
        jnp.asarray(row_turn),
        jnp.asarray(col_turn),
        steps,
        value_weight,
        inflow,
        readout,
        query_weight,
        key_weight,
        vector_weight,
        gate_weight,
        state_out,
        window_out,
    )


def streams(arrays):
    tokens, value, inflow, key, out = arrays[0], arrays[3], arrays[4], arrays[13], arrays[16]
    seats = lax.axis_size("sp")
    return (
        seats % 2 == 0
        and value.shape[0] % TILE == 0
        and out.shape[0] % value.shape[0] == 0
        and out.shape[1] == 2 * TILE
        and value.shape[1] == 4 * TILE
        and inflow.shape[1] * inflow.shape[2] == TILE
        and key.shape[1] == TILE
        and tokens.shape[0] == 6 * SSD_BLOCK
        and tokens.shape[1] == seats * value.shape[0]
        and seats == 2 * lax.axis_size("tp")
    )


def layer(*arrays):
    if streams(arrays):
        return streamed(*arrays)
    return shards(*arrays)


def shards(
    tokens,
    input_gain,
    gate_weight,
    value_weight,
    inflow_weight,
    readout_weight,
    step_weight,
    conv_values,
    conv_inflow,
    conv_readout,
    log_rate,
    group_gain,
    query_weight,
    key_weight,
    vector_weight,
    sink_logit,
    state_out,
    window_out,
):
    count = tokens.shape[0]
    offset = lax.axis_index("sp") * count
    seq_total = count * lax.axis_size("sp")
    heads = step_weight.shape[2]
    groups = inflow_weight.shape[1]
    state_len = inflow_weight.shape[2]
    inner_local = value_weight.shape[1]
    q_count = query_weight.shape[1] // HEAD_DIM
    kv_count = key_weight.shape[1] // HEAD_DIM
    kv_width = key_weight.shape[1]
    wide = tokens.astype(F32)
    normed = (
        wide
        * lax.rsqrt(jnp.mean(wide * wide, axis=1, keepdims=True) + EPS)
        * input_gain.astype(F32)
    ).astype(BF16)

    def whole(parts):
        return lax.all_gather(jnp.concatenate(parts, axis=1), "sp", axis=0, tiled=True)

    own = (flatten_rows(inflow_weight), flatten_rows(readout_weight), flatten_rows(step_weight))
    first_matrix = whole((value_weight,) + own)
    rest_matrix = whole((key_weight, vector_weight, gate_weight, query_weight))
    first = jnp.dot(normed, first_matrix, preferred_element_type=F32)
    rest = jnp.dot(normed, rest_matrix, preferred_element_type=F32).astype(BF16)
    conv_width = inner_local + 2 * groups * state_len
    conv_input = first[:, :conv_width].astype(BF16)
    step = jax.nn.softplus(first[:, conv_width:])
    keyvals = rest[:, : 2 * kv_width]
    gate = rest[:, 2 * kv_width : 2 * kv_width + inner_local]
    queries = rest[:, 2 * kv_width + inner_local :]

    reach_rows = CONV // 2
    padded = with_halo(conv_input, (("sp", 0),), CONV // 2).astype(F32)
    taps = jnp.concatenate(
        [conv_values, flatten_rows(conv_inflow), flatten_rows(conv_readout)], axis=1
    ).astype(F32)
    conv_sum = padded[0:count] * taps[0]
    for tap in range(1, 2 * reach_rows + 1):
        conv_sum = conv_sum + padded[tap : tap + count] * taps[tap]
    cells = jax.nn.silu(conv_sum).astype(BF16)
    rates = jnp.transpose(log_rate, (1, 0, 2)).reshape(count, 2 * heads)
    sd = jnp.concatenate([step, -jnp.exp(rates) * step], axis=1)
    blocks = count // SSD_BLOCK
    sdt = jnp.transpose(sd.reshape(blocks, SSD_BLOCK, 4 * heads), (0, 2, 1))

    summary = call(
        summary_kernel,
        jax.ShapeDtypeStruct((2, state_len + PAD, inner_local), BF16),
        (cells, sd),
    )
    everyone = lax.all_gather(summary, "sp")
    out_stack, everyone = lax.optimization_barrier(
        (jnp.concatenate([state_out, window_out], axis=0), everyone)
    )
    out_matrix = lax.all_gather(out_stack, "sp", axis=1, tiled=True)
    seats = lax.axis_size("sp")
    place = lax.axis_index("sp")
    totals = everyone[:, :, state_len].astype(F32) + everyone[:, :, state_len + 1].astype(F32)
    seat = jnp.arange(seats)
    starts = []
    for e in range(2):
        ahead = seat < place if e == 0 else seat > place
        between = (seat[None, :] > seat[:, None]) if e == 0 else (seat[None, :] < seat[:, None])
        between = (between & ahead[None, :])[:, :, None]
        fade = jnp.sum(jnp.where(between, totals[None, :, e], 0.0), axis=1)
        fade = jnp.where(ahead[:, None], jnp.exp(fade), 0.0)
        starts.append(jnp.sum(fade[:, None, :] * everyone[:, e, :state_len].astype(F32), axis=0))
    starts = jnp.stack(starts)
    state_features = call(
        mixer_kernel,
        jax.ShapeDtypeStruct((count, inner_local), BF16),
        (cells, sd, sdt, starts, gate, group_gain[None]),
        (
            pltpu.VMEM((blocks, state_len, inner_local), BF16),
            pltpu.VMEM((state_len, inner_local), F32),
        ),
        flops=10**10,
    )

    beside = with_halo(keyvals, (("sp", 0),), WINDOW)
    quarter = HEAD_DIM // 4
    freqs = ROPE_BASE ** (-jnp.arange(quarter).astype(F32) / quarter)
    spots = offset - WINDOW + jnp.arange(count + 2 * WINDOW, dtype=jnp.int32)
    row_angle = (spots // GRID_W).astype(F32)[:, None] * freqs
    col_angle = (spots % GRID_W).astype(F32)[:, None] * freqs
    angles = jnp.concatenate([row_angle, col_angle], axis=1)
    cosine = jnp.cos(angles)
    sine = jnp.sin(angles)

    def doubled(table, sign):
        low = table[:, :quarter]
        high = table[:, quarter:]
        return [sign * low, low, sign * high, high]

    turn = jnp.concatenate(doubled(cosine, 1.0) + doubled(sine, -1.0), axis=1)
    channel = jnp.arange(HEAD_DIM)
    partner = channel + jnp.where(channel % (2 * quarter) < quarter, quarter, -quarter)
    swap = (channel[:, None] == partner[None, :]).astype(BF16)
    limits = jnp.stack([offset, seq_total]).astype(jnp.int32)
    window_features, log_total = call(
        attend_kernel,
        (
            jax.ShapeDtypeStruct((count, q_count * HEAD_DIM), BF16),
            jax.ShapeDtypeStruct((count, q_count), F32),
        ),
        (limits, sink_logit, queries, beside, turn, swap),
        (pltpu.VMEM((kv_count, count + 2 * WINDOW, HEAD_DIM), BF16),),
        scalars=2,
        flops=10**10,
    )
    features = jnp.concatenate([state_features, window_features], axis=1)
    terms = jnp.dot(features, out_matrix, preferred_element_type=F32)
    mixed = lax.psum_scatter(terms.astype(BF16), "tp", scatter_dimension=1, tiled=True)
    return (mixed, log_total)


def solution(mesh):
    placed = (
        P("sp", None),
        P(),
        P("sp", "tp"),
        P("sp", "tp"),
        P("sp", "tp", None),
        P("sp", "tp", None),
        P("sp", None, "tp"),
        P(None, "tp"),
        P(None, "tp", None),
        P(None, "tp", None),
        P(None, "sp", "tp"),
        P("tp"),
        P("sp", "tp"),
        P("sp", "tp"),
        P("sp", "tp"),
        P("tp"),
        P("tp", "sp"),
        P("tp", "sp"),
    )
    return jax.shard_map(
        layer,
        mesh=mesh,
        in_specs=placed,
        out_specs=(P("sp", "tp"), P("sp", "tp")),
        check_vma=False,
    )
```

profile of v0, /device:TPU:0, one launch (start us, length us, event | category | flops | bytes accessed | tf_op | source)
XLA Modules:
  0.0 195.5 jit_solution(9167086172039520118)
XLA Ops:
  0.6 1.2 broadcast_in_dim.7.norm_gain_ref
  1.9 1.3 broadcast_in_dim.6.gain_ref
  3.2 1.3 pad_maximum_fusion.taps_ref
  4.5 0.8 negate_bitcast_fusion
  5.3 0.2 copy.24
  5.5 0.8 pad.4.rates_ref
  6.3 185.4 %shard_map.203 = (bf16[768,512]{1,0:T(8,128)(2,1)}, f32[768,8]{1,0:T(8,128)}) custom-call(bf16[768,2048]{1,0:T(8,128)(2,1)} %tokens_ref.1, bf16[1,2048]{1,0:T(2,128)(2,1)} %broadcast_in_dim.6.gain_ref, bf16[5,768]{1,0:T(8,128)(2,1)} %pad_maximum_fusion.taps_ref, f32[768,128]{1,0:T(8,128)} %pad.4.rates_ref, bf16[1,512]{1,0:T(2,128)(2,1)} %broadcast_in_dim.7.norm_gain_ref, ...), custom_call_target="tpu_custom_call" | custom-call | tf_op jit(solution)/shard_map/pallas_call | solution.py:1046
  191.7 1.7 copy.25
  193.4 2.1 %copy.27 = bf16[768,512]{1,0:T(8,128)(2,1)} copy(bf16[768,512]{1,0:T(8,128)(2,1)} %get-tuple-element.8) | data formatting | bytes 1572864
where the time goes:
time: 197 us; the launch traced here: 195 us
  Pallas kernels  185 us (94%)
  local copies, waits for them, and re-layouts  7.27 us (4%)
  other arithmetic  2.15 us (1%)
    pallas_call x1, Pallas kernels, streamed(): pl.pallas_call(functools.partial(layer_kernel, (seats, peers, units)), ou...  185 us

commit v1 on v0

--- a/solution.py
+++ b/solution.py
@@ -289,11 +289,12 @@
 
 def layer_kernel(
     cfg,
-    tokens_ref,
-    gain_ref,
-    taps_ref,
+    tokens_hbm,
+    gains_ref,
+    value_taps_ref,
+    inflow_taps_ref,
+    readout_taps_ref,
     rates_ref,
-    norm_gain_ref,
     sink_ref,
     row_turn_ref,
     col_turn_ref,
@@ -311,11 +312,11 @@
     log_ref,
     ring_ref,
     steps_all_ref,
+    tokens_ref,
     normed_ref,
     conv_ref,
     cells_ref,
     step_ref,
-    decay_ref,
     cum_ref,
     entry_ref,
     before_ref,
@@ -325,6 +326,7 @@
     scan_recv_ref,
     start_ref,
     reach_ref,
+    pair_ref,
     gate_ref,
     q_ref,
     kv_ref,
@@ -332,7 +334,8 @@
     turn_ref,
     feat_ref,
     part_ref,
-    peer_ref,
+    near_ref,
+    far_ref,
     send_sem,
     recv_sem,
     steps_send,
@@ -344,11 +347,13 @@
     kv_recv,
     scan_ssem,
     scan_rsem,
-    out_send,
-    out_recv,
+    near_send,
+    near_recv,
+    far_send,
+    far_recv,
 ):
     seats, peers, units = cfg
-    count, _ = tokens_ref.shape
+    count, width = tokens_hbm.shape
     unit_rows = ring_ref.shape[3]
     heads = steps_ref.shape[0] // 2
     wide = heads * HEAD_DIM
@@ -409,6 +414,8 @@
             )
     for copy in locals_:
         copy.start()
+    tokens_in = pltpu.make_async_copy(tokens_hbm, tokens_ref, local_sem.at[2 * per_dir])
+    tokens_in.start()
     steps_all_ref[place] = steps_ref[...]
     for copy in locals_:
         copy.wait()
@@ -458,13 +465,15 @@
         base = clock[0]
 
         def run(i, _):
-            for j in range(per_trip):
-                tick(base + i * per_trip + j)
+            for j in range(int(per_trip)):
+                tick(base + i * int(per_trip) + j)
+            if per_trip == 0.5:
+                pl.when(lax.rem(i, 2) == 0)(lambda: tick(base + lax.div(i, 2)))
             body(i)
             return 0
 
         lax.fori_loop(0, trips, run, 0)
-        clock[0] = base + trips * per_trip
+        clock[0] = base + (trips + 1) // 2 if per_trip == 0.5 else base + trips * per_trip
 
     def until(goal):
         if goal > clock[0]:
@@ -477,9 +486,10 @@
         rows = rows_at(b, size)
         x = tokens_ref[rows, :].astype(F32)
         scale = lax.rsqrt(jnp.mean(x * x, axis=1, keepdims=True) + EPS)
-        normed_ref[rows, :] = (x * scale * gain_ref[...].astype(F32)).astype(BF16)
-
-    sweep(blocks, 0, normalise)
+        normed_ref[rows, :] = (x * scale * gains_ref[:, :width].astype(F32)).astype(BF16)
+
+    tokens_in.wait()
+    sweep(blocks, 1, normalise)
     table_row = place * (count // GRID_W)
 
     def fill_turn(i):
@@ -575,7 +585,9 @@
 
     conv_edges = edge_copies(conv_ref, PAD, halo_send, halo_recv)
     edges_start(conv_edges)
-    decay_ref[...] = rates_ref[...] * step_ref[...]
+    taps = jnp.concatenate(
+        [ref[...] for ref in (value_taps_ref, inflow_taps_ref, readout_taps_ref)], axis=1
+    ).astype(F32)
     lane = iota((size, TILE), 1)
     row = iota((size, size), 0)
     col = iota((size, size), 1)
@@ -587,25 +599,26 @@
 
     def sums(b):
         rows = rows_at(b, size)
-        decay = decay_ref[rows, :]
+        filler = jnp.zeros((TILE - 2 * heads, size), F32)
+        rates = jnp.concatenate([rates_ref[0, :, rows], rates_ref[1, :, rows], filler], axis=0).T
+        decay = -jnp.exp(rates) * step_ref[rows, :]
         cum_ref[rows, :] = jnp.where(
             lane < heads, through(lower, decay, False), through(upper, decay, False)
         )
 
-    sweep(blocks, 0, sums)
+    sweep(blocks, 1, sums)
     edges_arrive(conv_edges)
 
     def convolve(b):
         rows = rows_at(b, size)
         padded = conv_ref[pl.ds(pl.multiple_of(b * size, size), size + 2 * PAD), :].astype(F32)
         first = PAD - CONV // 2
-        taps = taps_ref[...].astype(F32)
         total = padded[first : first + size] * taps[0:1]
         for tap in range(1, CONV):
             total = total + padded[first + tap : first + tap + size] * taps[tap : tap + 1]
         cells_ref[rows, :] = (total * jax.nn.sigmoid(total)).astype(BF16)
 
-    sweep(blocks, 1, convolve)
+    sweep(blocks, 0.5, convolve)
 
     def summarise(i):
         for e in range(2):
@@ -622,55 +635,84 @@
             carry_ref[e] = jnp.exp(edges[0:1]) * carry_ref[e] + fresh
             total_ref[e] = total_ref[e] + edges
 
-    sweep(blocks, 2, summarise)
-
-    jumps = [1]
-    while sum(jumps) < hops:
-        jumps.append(sum(jumps))
-
-    def scan_copy(r, e):
-        step = jumps[r] if e == 0 else seats - jumps[r]
+    sweep(blocks, 0.5, summarise)
+
+    pair = lax.div(place, 2)
+    pairs = seats // 2
+
+    def scan_copy(stage, e):
+        far = place + 1 - 2 * odd if stage == 0 else lax.rem(place + (2 if e == 0 else seats - 2), seats)
         return pltpu.make_async_remote_copy(
-            src_ref=scan_send_ref.at[e, r],
-            dst_ref=scan_recv_ref.at[e, r],
-            send_sem=scan_ssem.at[e, r],
-            recv_sem=scan_rsem.at[e, r],
-            device_id={"sp": lax.rem(place + step, seats)},
+            src_ref=scan_send_ref.at[e, stage],
+            dst_ref=scan_recv_ref.at[e, stage],
+            send_sem=scan_ssem.at[e, stage],
+            recv_sem=scan_rsem.at[e, stage],
+            device_id={"sp": far},
             device_id_type=mesh_id,
         )
 
-    def sends_to(r, e):
-        return place < seats - jumps[r] if e == 0 else place >= jumps[r]
-
-    def hears_from(r, e):
-        return place >= jumps[r] if e == 0 else place < seats - jumps[r]
-
-    def scan_start(r, state_ref, decay_sum_ref):
+    def scan_start(stage, e, states, total):
+        scan_send_ref[e, stage, :state] = states.astype(BF16)
+        high = total.astype(BF16).astype(F32)
+        at = iota((PAD, wide), 0)
+        scan_send_ref[e, stage, state:] = jnp.where(
+            at == 0, high, jnp.where(at == 1, total - high, 0.0)
+        ).astype(BF16)
+        scan_copy(stage, e).start()
+
+    def scan_read(stage, e):
+        far = scan_recv_ref[e, stage]
+        decays = far[state : state + 8].astype(F32)
+        return far[:state].astype(F32), decays[0:1] + decays[1:2]
+
+    def scan_pair():
         for e in range(2):
-            scan_send_ref[e, r, :state] = state_ref[e].astype(BF16)
-            total = decay_sum_ref[e][0:1]
-            high = total.astype(BF16).astype(F32)
-            at = iota((PAD, wide), 0)
-            scan_send_ref[e, r, state:] = jnp.where(
-                at == 0, high, jnp.where(at == 1, total - high, 0.0)
-            ).astype(BF16)
-            pl.when(sends_to(r, e))(lambda: scan_copy(r, e).start())
-
-    def scan_take(r):
+            scan_copy(0, e).wait_recv()
+            states, total = scan_read(0, e)
+            mine, my_total = carry_ref[e], total_ref[e][0:1]
+
+            @pl.when(odd == 1 - e)
+            def _():
+                pair_ref[e] = states * jnp.exp(my_total) + mine
+
+            @pl.when(odd == e)
+            def _():
+                pair_ref[e] = mine * jnp.exp(total) + states
+
+            total_ref[e] = total_ref[e] + total
+
+    def scan_slot(r):
         for e in range(2):
 
-            @pl.when(hears_from(r, e))
+            @pl.when(pair == (r if e == 0 else pairs - 1 - r))
             def _():
-                scan_copy(r, e).wait_recv()
-                far = scan_recv_ref[e, r]
-                decays = far[state : state + 8].astype(F32)
-                far_total = decays[0:1] + decays[1:2]
-                start_ref[e] = (
-                    far[:state].astype(F32) * jnp.exp(reach_ref[e][0:1]) + start_ref[e]
-                )
-                reach_ref[e] = reach_ref[e] + far_total
-
-    scan_start(0, carry_ref, total_ref)
+                if r > 0:
+                    scan_copy(1, e).wait_recv()
+                    states, total = scan_read(1, e)
+                    start_ref[e] = states
+                    reach_ref[e] = jnp.broadcast_to(total, reach_ref.shape[1:])
+                if r < pairs - 1:
+                    total = total_ref[e][0:1]
+                    scan_start(
+                        1, e, start_ref[e] * jnp.exp(total) + pair_ref[e], reach_ref[e][0:1] + total
+                    )
+
+    def scan_finish():
+        for e in range(2):
+
+            @pl.when(odd == 1 - e)
+            def _():
+                states, total = scan_read(0, e)
+                start_ref[e] = start_ref[e] * jnp.exp(total) + states
+
+    def scan_left():
+        for e in range(2):
+            scan_copy(0, e).wait_send()
+            goes = pair < pairs - 1 if e == 0 else pair > 0
+            pl.when(goes)(lambda: scan_copy(1, e).wait_send())
+
+    for e in range(2):
+        scan_start(0, e, carry_ref[e], total_ref[e][0:1])
 
     until(GROUP * hops * -(-(first_units + second_units) // GROUP))
 
@@ -689,8 +731,8 @@
     sweep(count // dot_rows, 1, second_dot_b)
     kv_edges = edge_copies(kv_ref, WINDOW, kv_send, kv_recv)
     edges_start(kv_edges)
-    scan_take(0)
-    scan_start(1, start_ref, reach_ref)
+    scan_pair()
+    scan_slot(0)
 
     def second_dot_a(b):
         rows = rows_at(b, dot_rows)
@@ -710,8 +752,6 @@
         other = jnp.where(low, pltpu.roll(x, TILE - quarter, 1), pltpu.roll(x, quarter, 1))
         return (x * table[:, :TILE] + other * table[:, TILE:]).astype(BF16)
 
-    edges_arrive(kv_edges)
-
     def prepare(b):
         rows = rows_at(b, size)
         for c in range(kv_width // TILE):
@@ -719,32 +759,34 @@
                 kv_ref[rows, c * TILE : (c + 1) * TILE], turn_ref[rows, :]
             )
 
-    sweep(kv_ref.shape[0] // size, 0, prepare)
+    sweep(blocks, 0, lambda i: prepare(i + 1))
 
     band = size + 2 * WINDOW
     band_row = iota((size, band), 0)
     band_col = iota((size, band), 1)
     near = (band_col >= band_row) & (band_col - band_row <= 2 * WINDOW)
-    q_lane = iota((size, q_count), 1)
+    q_lane = iota((size, TILE), 1)
     repeat = q_count * HEAD_DIM // kv_width
     seq_total = seats * count
-    later = [1, 3, 5]
-
-    def attend(b):
-        for r in range(1, len(jumps)):
-
-            @pl.when(b == later[r - 1])
-            def _():
-                scan_take(r)
-                if r + 1 < len(jumps):
-                    scan_start(r + 1, start_ref, reach_ref)
-
+    slots = {1: 1, 2: blocks - 2}
+
+    def attend(i):
+        for r in range(1, min(3, pairs)):
+            pl.when(i == slots[r])(lambda: scan_slot(r))
+
+        @pl.when(i == blocks - 2)
+        def _():
+            edges_arrive(kv_edges)
+            prepare(0)
+            prepare(blocks + 1)
+
+        b = lax.rem(i + 1, blocks)
         start = pl.multiple_of(b * size, size)
         rows = pl.ds(start, size)
         reach = pl.ds(start, band)
         key_pos = place * count + start - WINDOW + band_col
         valid = near & (key_pos >= 0) & (key_pos < seq_total)
-        logs = jnp.zeros((size, q_count), F32)
+        logs = jnp.zeros((size, TILE), F32)
         table = turn_ref[pl.ds(start + WINDOW, size), :]
         turned_q = jnp.concatenate(
             [turned(q_ref[rows, c * TILE : (c + 1) * TILE], table) for c in range(q_width // TILE)],
@@ -771,9 +813,9 @@
             outs.append((values / total).astype(BF16))
             logs = jnp.where(q_lane == h, top + jnp.log(total), logs)
         feat_ref[rows, wide:] = jnp.concatenate(outs, axis=1)
-        log_ref[rows, :] = logs
-
-    sweep(blocks, 3, attend)
+        log_ref[:, rows] = logs.T[:q_count]
+
+    sweep(blocks, 2, attend)
 
     gate_first = first_units + second_units
     until(GROUP * hops * -(-(gate_first + gate_units) // GROUP))
@@ -787,7 +829,10 @@
                 preferred_element_type=F32,
             ).astype(BF16)
 
-    sweep(count // dot_rows, 0, gate_dot)
+    sweep(count // dot_rows, 1, gate_dot)
+    for r in range(3, pairs):
+        scan_slot(r)
+    scan_finish()
 
     def mix(b):
         rows = rows_at(b, size)
@@ -821,28 +866,49 @@
         gate = gate_ref[rows, :].astype(F32)
         y = y * (gate * jax.nn.sigmoid(gate))
         y = y * lax.rsqrt(jnp.mean(y * y, axis=1, keepdims=True) + EPS)
-        feat_ref[rows, :wide] = (y * norm_gain_ref[...].astype(F32)).astype(BF16)
-
-    left_ticks = sends - GROUP - clock[0]
-    sweep(blocks, min(2, left_ticks // blocks), mix)
+        feat_ref[rows, :wide] = (y * gains_ref[:, width:].astype(F32)).astype(BF16)
+
+    sweep(blocks, 1, mix)
 
     out_first = gate_first + gate_units
     out_units = per_dir - out_first
     per_peer = 2 * seats // peers
 
-    def out_copy(tile):
-        dest = lax.div(tile, per_peer)
-        return dest, pltpu.make_async_remote_copy(
-            src_ref=part_ref.at[tile],
-            dst_ref=peer_ref.at[lane_peer, lax.rem(tile, per_peer)],
-            send_sem=out_send.at[tile],
-            recv_sem=out_recv.at[lane_peer, lax.rem(tile, per_peer)],
+    dot_blocks = count // dot_rows
+
+    core = lax.rem(lane_peer, 2)
+    beside = lane_peer + 1 - 2 * core
+
+    def near_copy(tile, b):
+        rows = rows_at(b, dot_rows)
+        return pltpu.make_async_remote_copy(
+            src_ref=part_ref.at[tile, rows],
+            dst_ref=near_ref.at[tile, rows],
+            send_sem=near_send.at[tile, b],
+            recv_sem=near_recv.at[tile, b],
+            device_id={"tp": beside},
+            device_id_type=mesh_id,
+        )
+
+    def far_copy(tile, b, dest, slot):
+        rows = rows_at(b, dot_rows)
+        at = lax.rem(tile, per_peer)
+        return pltpu.make_async_remote_copy(
+            src_ref=part_ref.at[tile, rows],
+            dst_ref=far_ref.at[slot, at, rows],
+            send_sem=far_send.at[tile, b],
+            recv_sem=far_recv.at[slot, at, b],
             device_id={"tp": dest},
             device_id_type=mesh_id,
         )
 
+    def dest_of(tile):
+        dest = lax.div(tile, per_peer)
+        return dest, lax.rem(dest, 2) == core, lax.div(dest, 2) == lax.div(lane_peer, 2)
+
     def project(d, owner):
         tile = 2 * owner + d
+        _, kept, _ = dest_of(tile)
         matrix = ring_ref[d, out_first:, owner].reshape(out_units * unit_rows, TILE)
 
         def rows_dot(b, _):
@@ -850,63 +916,85 @@
             part_ref[tile, rows, :] = jnp.dot(
                 feat_ref[rows, :], matrix, preferred_element_type=F32
             ).astype(BF16)
+            pl.when(jnp.logical_not(kept))(lambda: near_copy(tile, b).start())
             return 0
 
-        lax.fori_loop(0, count // dot_rows, rows_dot, 0)
-        dest, copy = out_copy(tile)
-        pl.when(dest != lane_peer)(lambda: copy.start())
-
-    for d in range(2):
-        project(d, place)
+        lax.fori_loop(0, dot_blocks, rows_dot, 0)
+
+    def join(d, owner):
+        tile = 2 * owner + d
+        dest, kept, local = dest_of(tile)
+
+        @pl.when(kept)
+        def _():
+            def rows_add(b, _):
+                rows = rows_at(b, dot_rows)
+                near_copy(tile, b).wait_recv()
+                part_ref[tile, rows, :] = (
+                    part_ref[tile, rows, :].astype(F32) + near_ref[tile, rows, :].astype(F32)
+                ).astype(BF16)
+
+                @pl.when(jnp.logical_not(local))
+                def _():
+                    far_copy(tile, b, dest, lax.div(lane_peer, 2)).start()
+
+                return 0
+
+            lax.fori_loop(0, dot_blocks, rows_add, 0)
+
     final = sends - GROUP * hops
-    done = max(0, (clock[0] - final) // GROUP)
+    limit = sends - GROUP
+
+    def project_own(_):
+        for d in range(2):
+            project(d, place)
+
+    def ready():
+        return min(hops - 1, max(0, (clock[0] - final) // GROUP))
+
+    sweep(1, min(1, limit - clock[0]), project_own)
 
     def project_hop(k):
         project(0, seat_at(my_pos - k - 1))
         project(1, seat_at(my_pos + k + 1))
-
-    def early(k, _):
-        project_hop(k)
-        return 0
-
-    lax.fori_loop(0, done, early, 0)
+        join(0, seat_at(my_pos - k))
+        join(1, seat_at(my_pos + k))
+
+    done = 0
+    while ready() > done:
+        first, more = done, ready() - done
+        sweep(more, 1 if clock[0] + more <= limit else 0, lambda i: project_hop(i + first))
+        done = first + more
+    if done < hops - 1 and clock[0] > final + GROUP * done:
+        until(final + GROUP * (done + 1))
+        project_hop(jnp.int32(done))
+        done += 1
     until(final + GROUP * done)
     sweep(hops - 1 - done, GROUP, lambda i: project_hop(i + done))
     for j in range(GROUP):
         tick(jnp.int32(sends - GROUP + j), last=True)
     project_hop(jnp.int32(hops - 1))
-
-    def gather_peers(r, _):
-        source = lax.rem(lane_peer + r, peers)
-        for j in range(per_peer):
-            pltpu.make_async_remote_copy(
-                src_ref=part_ref.at[j],
-                dst_ref=peer_ref.at[source, j],
-                send_sem=out_send.at[j],
-                recv_sem=out_recv.at[source, j],
-                device_id={"tp": source},
-                device_id_type=mesh_id,
-            ).wait_recv()
-        return 0
-
-    lax.fori_loop(1, peers, gather_peers, 0)
+    join(0, seat_at(my_pos - hops))
+    join(1, seat_at(my_pos + hops))
+
+    chips = peers // 2
 
     def add_up(b, _):
-        rows = rows_at(b, size)
+        rows = rows_at(b, dot_rows)
         for j in range(per_peer):
             total = part_ref[lane_peer * per_peer + j, rows, :].astype(F32)
-            for r in range(1, peers):
-                total = total + peer_ref[lax.rem(lane_peer + r, peers), j, rows, :].astype(F32)
+            for r in range(1, chips):
+                slot = lax.rem(lax.div(lane_peer, 2) + r, chips)
+                far_copy(jnp.int32(j), b, 2 * slot + core, slot).wait_recv()
+                total = total + far_ref[slot, j, rows, :].astype(F32)
             out_ref[rows, j * TILE : (j + 1) * TILE] = total.astype(BF16)
         return 0
 
-    lax.fori_loop(0, blocks, add_up, 0)
+    lax.fori_loop(0, dot_blocks, add_up, 0)
 
     edges_left(conv_edges)
     edges_left(kv_edges)
-    for r in range(len(jumps)):
-        for e in range(2):
-            pl.when(sends_to(r, e))(lambda: scan_copy(r, e).wait_send())
+    scan_left()
     for r in range(1, seats):
         steps_copy(r).wait_send()
 
@@ -918,8 +1006,18 @@
     lax.fori_loop(0, sends, ring_left, 0)
 
     def out_left(tile, _):
-        dest, copy = out_copy(tile)
-        pl.when(dest != lane_peer)(lambda: copy.wait_send())
+        dest, kept, local = dest_of(tile)
+
+        @pl.when(jnp.logical_not(kept))
+        def _():
+            for b in range(dot_blocks):
+                near_copy(tile, b).wait_send()
+
+        @pl.when(kept & jnp.logical_not(local))
+        def _():
+            for b in range(dot_blocks):
+                far_copy(tile, b, dest, lax.div(lane_peer, 2)).wait_send()
+
         return 0
 
     lax.fori_loop(0, 2 * seats, out_left, 0)
@@ -977,9 +1075,6 @@
     q_width = query_weight.shape[1]
     kv_width = key_weight.shape[1]
     blocks = count // SSD_BLOCK
-    taps = jnp.concatenate([conv_values, flatten_rows(conv_inflow), flatten_rows(conv_readout)], axis=1)
-    rates = -jnp.exp(jnp.transpose(log_rate, (1, 0, 2)).reshape(count, 2 * heads))
-    rates = jnp.pad(rates, ((0, 0), (0, TILE - 2 * heads)))
     steps = jnp.transpose(step_weight, (1, 2, 0)).reshape(2 * heads, unit_rows)
     row_turn, col_turn = turn_tables(seats * count // GRID_W)
     units = chunk_maps(
@@ -997,9 +1092,6 @@
     )
     per_dir = len(units[0])
     sends = per_dir * (seats - 1)
-    rounds = 1
-    while 2 ** (rounds - 1) < seats - 1:
-        rounds += 1
     vmem = pl.BlockSpec(memory_space=pltpu.VMEM)
     smem = pl.BlockSpec(memory_space=pltpu.SMEM)
     hbm = pl.BlockSpec(memory_space=pltpu.HBM)
@@ -1008,19 +1100,20 @@
         pltpu.VMEM((2, per_dir, seats, unit_rows, TILE), BF16),
         pltpu.VMEM((seats, 2 * heads, unit_rows), BF16),
         pltpu.VMEM((count, width), BF16),
+        pltpu.VMEM((count, width), BF16),
         pltpu.VMEM((count + 2 * PAD, conv_width), BF16),
         pltpu.VMEM((count, conv_width), BF16),
-        pltpu.VMEM((count, TILE), F32),
         pltpu.VMEM((count, TILE), F32),
         pltpu.VMEM((count, TILE), F32),
         pltpu.VMEM((2, blocks, state, wide), F32),
         pltpu.VMEM((2, blocks, 8, wide), F32),
         pltpu.VMEM((2, state, wide), F32),
         pltpu.VMEM((2, 8, wide), F32),
-        pltpu.VMEM((2, rounds, state + PAD, wide), BF16),
-        pltpu.VMEM((2, rounds, state + PAD, wide), BF16),
+        pltpu.VMEM((2, 2, state + PAD, wide), BF16),
+        pltpu.VMEM((2, 2, state + PAD, wide), BF16),
         pltpu.VMEM((2, state, wide), F32),
         pltpu.VMEM((2, 8, wide), F32),
+        pltpu.VMEM((2, state, wide), F32),
         pltpu.VMEM((count, wide), BF16),
         pltpu.VMEM((count, q_width), BF16),
         pltpu.VMEM((count + 2 * WINDOW, 2 * kv_width), BF16),
@@ -1028,28 +1121,31 @@
         pltpu.VMEM((count + 2 * WINDOW, 2 * TILE), F32),
         pltpu.VMEM((count, wide + q_width), BF16),
         pltpu.VMEM((2 * seats, count, TILE), BF16),
-        pltpu.VMEM((peers, 2 * seats // peers, count, TILE), BF16),
+        pltpu.VMEM((2 * seats, count, TILE), BF16),
+        pltpu.VMEM((peers // 2, 2 * seats // peers, count, TILE), BF16),
         dma((2, sends)),
         dma((2, sends)),
         dma((seats,)),
         dma((seats,)),
-        dma((2 * per_dir,)),
+        dma((2 * per_dir + 1,)),
         dma((2,)),
         dma((2,)),
         dma((2,)),
         dma((2,)),
-        dma((2, rounds)),
-        dma((2, rounds)),
-        dma((2 * seats,)),
-        dma((peers, 2 * seats // peers)),
+        dma((2, 2)),
+        dma((2, 2)),
+        dma((2 * seats, count // (2 * SSD_BLOCK))),
+        dma((2 * seats, count // (2 * SSD_BLOCK))),
+        dma((2 * seats, count // (2 * SSD_BLOCK))),
+        dma((peers // 2, 2 * seats // peers, count // (2 * SSD_BLOCK))),
     ]
-    return pl.pallas_call(
+    mixed, logs = pl.pallas_call(
         functools.partial(layer_kernel, (seats, peers, units)),
         out_shape=(
             jax.ShapeDtypeStruct((count, width // peers), BF16),
-            jax.ShapeDtypeStruct((count, q_width // HEAD_DIM), F32),
+            jax.ShapeDtypeStruct((q_width // HEAD_DIM, count), F32),
         ),
-        in_specs=[vmem] * 5 + [smem] + [vmem] * 3 + [hbm] * 9,
+        in_specs=[hbm] + [vmem] * 5 + [smem] + [vmem] * 3 + [hbm] * 9,
         out_specs=(vmem, vmem),
         scratch_shapes=scratch,
         compiler_params=pltpu.CompilerParams(
@@ -1057,10 +1153,11 @@
         ),
     )(
         tokens,
-        input_gain[None],
-        taps,
-        rates,
-        group_gain[None],
+        jnp.concatenate([input_gain, group_gain])[None],
+        conv_values,
+        flatten_rows(conv_inflow),
+        flatten_rows(conv_readout),
+        jnp.transpose(log_rate, (0, 2, 1)),
         sink_logit,
         jnp.asarray(row_turn),
         jnp.asarray(col_turn),
@@ -1075,6 +1172,7 @@
         state_out,
         window_out,
     )
+    return mixed, logs.T
 
 
 def streams(arrays):
@@ -1088,7 +1186,9 @@
         and value.shape[1] == 4 * TILE
         and inflow.shape[1] * inflow.shape[2] == TILE
         and key.shape[1] == TILE
-        and tokens.shape[0] == 6 * SSD_BLOCK
+        and tokens.shape[0] % (2 * SSD_BLOCK) == 0
+        and tokens.shape[0] >= 4 * SSD_BLOCK
+        and tokens.shape[0] % GRID_W == 0
         and tokens.shape[1] == seats * value.shape[0]
         and seats == 2 * lax.axis_size("tp")
     )

time: 197 us -> 169 us (0.86)
  Pallas kernels: 185 us -> 164 us
  local copies, waits for them, and re-layouts: 7.27 us -> 4.02 us
    pallas_call x1, Pallas kernels: 185 us -> 164 us  [streamed(): pl.pallas_call(functools.partial(layer_kernel, (seats, peers, units)), ou...]
where the time goes in v1:
time: 169 us
  Pallas kernels  164 us (97%)
  local copies, waits for them, and re-layouts  4.02 us (2%)
    pallas_call x1, Pallas kernels, streamed(): pl.pallas_call(functools.partial(layer_kernel, (seats, peers, units)), ou...  164 us
    unnamed x2, local copies, waits for them, and re-layouts  3.41 us

profile of v1, /device:TPU:0, one launch (start us, length us, event | category | flops | bytes accessed | tf_op | source)
XLA Modules:
  0.0 169.0 jit_solution(8786864482298310907)
XLA Ops:
  0.6 0.7 pad_maximum_fusion
  1.3 0.6 broadcast_in_dim.3.gains_ref
  1.9 163.6 %shard_map.203 = (bf16[768,512]{1,0:T(8,128)(2,1)}, f32[8,768]{1,0:T(8,128)}) custom-call(bf16[768,2048]{1,0:T(8,128)(2,1)} %tokens_hbm.1, bf16[1,2560]{1,0:T(2,128)(2,1)} %broadcast_in_dim.3.gains_ref, bf16[5,512]{1,0:T(8,128)(2,1)} %value_taps_ref.1, bf16[5,128]{1,0:T(8,128)(2,1)} %bitcast.14, bf16[5,128]{1,0:T(8,128)(2,1)} %bitcast.15, ...), custom_call_target="tpu_custom_call" | custom-call | tf_op jit(solution)/shard_map/pallas_call | solution.py:1142
  165.6 2.1 %copy.24 = bf16[768,512]{1,0:T(8,128)(2,1)} copy(bf16[768,512]{1,0:T(8,128)(2,1)} %get-tuple-element.8) | data formatting | bytes 1572864
  167.7 1.3 copy.25

commit v2 on v1

--- a/solution.py
+++ b/solution.py
@@ -290,7 +290,8 @@
 def layer_kernel(
     cfg,
     tokens_hbm,
-    gains_ref,
+    gain_ref,
+    norm_gain_ref,
     value_taps_ref,
     inflow_taps_ref,
     readout_taps_ref,
@@ -417,8 +418,9 @@
     tokens_in = pltpu.make_async_copy(tokens_hbm, tokens_ref, local_sem.at[2 * per_dir])
     tokens_in.start()
     steps_all_ref[place] = steps_ref[...]
-    for copy in locals_:
-        copy.wait()
+    first_ones = [d * per_dir + u for d in range(2) for u in range(GROUP)]
+    for at in first_ones:
+        locals_[at].wait()
     pl.semaphore_wait(barrier, hops + peers - 1)
 
     def ring_copy(i, d, behind):
@@ -446,6 +448,10 @@
         for d in range(2):
             ring_copy(jnp.int32(j), d, 0).start()
 
+    for at, copy in enumerate(locals_):
+        if at not in first_ones:
+            copy.wait()
+
     def steps_copy(r):
         return pltpu.make_async_remote_copy(
             src_ref=steps_ref,
@@ -486,7 +492,7 @@
         rows = rows_at(b, size)
         x = tokens_ref[rows, :].astype(F32)
         scale = lax.rsqrt(jnp.mean(x * x, axis=1, keepdims=True) + EPS)
-        normed_ref[rows, :] = (x * scale * gains_ref[:, :width].astype(F32)).astype(BF16)
+        normed_ref[rows, :] = (x * scale * gain_ref[...].astype(F32).reshape(1, width)).astype(BF16)
 
     tokens_in.wait()
     sweep(blocks, 1, normalise)
@@ -716,6 +722,8 @@
 
     until(GROUP * hops * -(-(first_units + second_units) // GROUP))
 
+    scan_pair()
+    scan_slot(0)
     q_last = second_units - 2 * kv_width // TILE
 
     def second_dot_b(b):
@@ -731,8 +739,6 @@
     sweep(count // dot_rows, 1, second_dot_b)
     kv_edges = edge_copies(kv_ref, WINDOW, kv_send, kv_recv)
     edges_start(kv_edges)
-    scan_pair()
-    scan_slot(0)
 
     def second_dot_a(b):
         rows = rows_at(b, dot_rows)
@@ -768,7 +774,7 @@
     q_lane = iota((size, TILE), 1)
     repeat = q_count * HEAD_DIM // kv_width
     seq_total = seats * count
-    slots = {1: 1, 2: blocks - 2}
+    slots = {1: 0, 2: blocks // 2}
 
     def attend(i):
         for r in range(1, min(3, pairs)):
@@ -866,7 +872,7 @@
         gate = gate_ref[rows, :].astype(F32)
         y = y * (gate * jax.nn.sigmoid(gate))
         y = y * lax.rsqrt(jnp.mean(y * y, axis=1, keepdims=True) + EPS)
-        feat_ref[rows, :wide] = (y * gains_ref[:, width:].astype(F32)).astype(BF16)
+        feat_ref[rows, :wide] = (y * norm_gain_ref[...].astype(F32).reshape(1, wide)).astype(BF16)
 
     sweep(blocks, 1, mix)
 
@@ -1040,6 +1046,11 @@
         return np.concatenate(one * copies + two * copies, axis=1).astype(np.float32)
 
     return table(row_angle, True), table(col_angle, False)
+
+
+def hand_on_kernel(mixed_ref, logs_ref, mixed_out_ref, logs_out_ref):
+    mixed_out_ref[...] = mixed_ref[...]
+    logs_out_ref[...] = logs_ref[...]
 
 
 def streamed(
@@ -1145,7 +1156,7 @@
             jax.ShapeDtypeStruct((count, width // peers), BF16),
             jax.ShapeDtypeStruct((q_width // HEAD_DIM, count), F32),
         ),
-        in_specs=[hbm] + [vmem] * 5 + [smem] + [vmem] * 3 + [hbm] * 9,
+        in_specs=[hbm] + [vmem] * 6 + [smem] + [vmem] * 3 + [hbm] * 9,
         out_specs=(vmem, vmem),
         scratch_shapes=scratch,
         compiler_params=pltpu.CompilerParams(
@@ -1153,7 +1164,8 @@
         ),
     )(
         tokens,
-        jnp.concatenate([input_gain, group_gain])[None],
+        input_gain,
+        group_gain,
         conv_values,
         flatten_rows(conv_inflow),
         flatten_rows(conv_readout),
@@ -1171,6 +1183,14 @@
         gate_weight,
         state_out,
         window_out,
+    )
+    mixed, logs = call(
+        hand_on_kernel,
+        (
+            jax.ShapeDtypeStruct(mixed.shape, mixed.dtype),
+            jax.ShapeDtypeStruct(logs.shape, logs.dtype),
+        ),
+        (mixed, logs),
     )
     return mixed, logs.T
 

time: 169 us -> 166 us (0.982)
  local copies, waits for them, and re-layouts: 4.02 us -> 1.86 us
    unnamed x2 -> x4, local copies, waits for them, and re-layouts: 3.41 us -> 1.86 us
where the time goes in v2:
time: 166 us
  Pallas kernels  163 us (98%)
  local copies, waits for them, and re-layouts  1.86 us (1%)
    pallas_call x1, Pallas kernels, streamed(): pl.pallas_call(functools.partial(layer_kernel, (seats, peers, units)), ou...  162 us

profile of v2, /device:TPU:0, one launch (start us, length us, event | category | flops | bytes accessed | tf_op | source)
XLA Modules:
  0.0 165.8 jit_solution(7721456086483380891)
XLA Ops:
  0.6 162.4 %shard_map.203 = (bf16[768,512]{1,0:T(8,128)(2,1)}, f32[8,768]{1,0:T(8,128)}) custom-call(bf16[768,2048]{1,0:T(8,128)(2,1)} %tokens_hbm.1, bf16[2048]{0:T(1024)(128)(2,1)} %gain_ref.1, bf16[512]{0:T(512)(128)(2,1)} %norm_gain_ref.1, bf16[5,512]{1,0:T(8,128)(2,1)} %value_taps_ref.1, bf16[5,128]{1,0:T(8,128)(2,1)} %bitcast.13, bf16[5,128]{1,0:T(8,128)(2,1)} %bitcast.14, ...), custom_call_target="tpu_custom_call" | custom-call | tf_op jit(solution)/shard_map/pallas_call | solution.py:1153
  163.0 0.0 copy-start
  163.0 1.1 copy-done
  164.2 0.0 copy-start.1
  164.2 0.7 copy-done.1
  164.9 0.9 shard_map.204
Async XLA Ops:
  163.0 1.1 copy-start
  164.2 0.7 copy-start.1

commit v3 on v2

--- a/solution.py
+++ b/solution.py
@@ -673,19 +673,22 @@
 
     def scan_pair():
         for e in range(2):
-            scan_copy(0, e).wait_recv()
-            states, total = scan_read(0, e)
-            mine, my_total = carry_ref[e], total_ref[e][0:1]
-
-            @pl.when(odd == 1 - e)
+
+            @pl.when(jnp.logical_not(spared(e, e)))
             def _():
-                pair_ref[e] = states * jnp.exp(my_total) + mine
-
-            @pl.when(odd == e)
-            def _():
-                pair_ref[e] = mine * jnp.exp(total) + states
-
-            total_ref[e] = total_ref[e] + total
+                scan_copy(0, e).wait_recv()
+                states, total = scan_read(0, e)
+                mine, my_total = carry_ref[e], total_ref[e][0:1]
+
+                @pl.when(odd == 1 - e)
+                def _():
+                    pair_ref[e] = states * jnp.exp(my_total) + mine
+
+                @pl.when(odd == e)
+                def _():
+                    pair_ref[e] = mine * jnp.exp(total) + states
+
+                total_ref[e] = total_ref[e] + total
 
     def scan_slot(r):
         for e in range(2):
@@ -713,12 +716,17 @@
 
     def scan_left():
         for e in range(2):
-            scan_copy(0, e).wait_send()
+            pl.when(jnp.logical_not(spared(e, 1 - e)))(lambda: scan_copy(0, e).wait_send())
             goes = pair < pairs - 1 if e == 0 else pair > 0
             pl.when(goes)(lambda: scan_copy(1, e).wait_send())
 
+    def spared(e, side):
+        return (pair == (pairs - 1 if e == 0 else 0)) & (odd == side)
+
     for e in range(2):
-        scan_start(0, e, carry_ref[e], total_ref[e][0:1])
+        pl.when(jnp.logical_not(spared(e, 1 - e)))(
+            lambda: scan_start(0, e, carry_ref[e], total_ref[e][0:1])
+        )
 
     until(GROUP * hops * -(-(first_units + second_units) // GROUP))
 

time: 166 us -> 165 us (level)
  no operation moved by 1% of the time
where the time goes in v3:
time: 165 us
  Pallas kernels  163 us (99%)
  local copies, waits for them, and re-layouts  1.86 us (1%)
    pallas_call x1, Pallas kernels, streamed(): pl.pallas_call(functools.partial(layer_kernel, (seats, peers, units)), ou...  162 us

profile of v3, /device:TPU:0, one launch (start us, length us, event | category | flops | bytes accessed | tf_op | source)
XLA Modules:
  0.0 165.1 jit_solution(10227260214758895713)
XLA Ops:
  0.6 161.6 %shard_map.203 = (bf16[768,512]{1,0:T(8,128)(2,1)}, f32[8,768]{1,0:T(8,128)}) custom-call(bf16[768,2048]{1,0:T(8,128)(2,1)} %tokens_hbm.1, bf16[2048]{0:T(1024)(128)(2,1)} %gain_ref.1, bf16[512]{0:T(512)(128)(2,1)} %norm_gain_ref.1, bf16[5,512]{1,0:T(8,128)(2,1)} %value_taps_ref.1, bf16[5,128]{1,0:T(8,128)(2,1)} %bitcast.13, bf16[5,128]{1,0:T(8,128)(2,1)} %bitcast.14, ...), custom_call_target="tpu_custom_call" | custom-call | tf_op jit(solution)/shard_map/pallas_call | solution.py:1161
  162.3 0.0 copy-start
  162.3 1.1 copy-done
  163.4 0.0 copy-start.1
  163.4 0.7 copy-done.1
  164.1 0.9 shard_map.204
Async XLA Ops:
  162.3 1.1 copy-start
  163.4 0.7 copy-start.1
